TPU v7x, 32 devices: a whole 2x2x4 slice. The times are simulated.
32 devices in a mesh: grp: 2 (over y), ep: 4 (over z), tp: 4 (over x, core).
Axes of the slice: x: 2, y: 2, z: 4, core: 2. Of those that a mesh axis runs over, the one named last changes fastest.
Arguments:
- queries: bfloat16 [2048, 1024], P(('grp', 'ep'), 'tp'), parts along dimension 0, may hold values from -6 to 6
- head_key_rows: bfloat16 [2048, 1024], P(('grp', 'ep'), 'tp'), parts along dimension 0, may hold values from -6 to 6
- head_value_rows: bfloat16 [2048, 2048], P(('grp', 'ep'), 'tp'), parts along dimension 0, may hold values from -6 to 6
- output_gate_logits: bfloat16 [2048, 2048], P(('grp', 'ep'), 'tp'), parts along dimension 0, may hold values from -6 to 6
- log_input_gate: float32 [4, 2048], P('tp', ('grp', 'ep')), parts along dimension 1, may hold values from -5 to 103
- forget_gate_logits: float32 [4, 2048], P('tp', ('grp', 'ep')), parts along dimension 1, may hold values from 1 to 20
- extra_log_forget: float32 [4, 2048], P('tp', ('grp', 'ep')), parts along dimension 1, may hold values from -1 to 0, as said below
- head_norm_gain: float32 [2048], P('tp'), may hold values from 0.1 to 1.9
- memory_output_matrix: bfloat16 [2048, 2048], P('tp'), may hold values from -0.125 to 0.125
- expert_input_tokens: bfloat16 [2048, 2048], P(('grp', 'ep', 'tp')), parts along dimension 0, may hold values from -6 to 6
- expert_norm_gain: float32 [2048], replicated, may hold values from 0.1 to 1.9
- routes: int32 [2048, 2], P(('grp', 'ep', 'tp')), parts along dimension 0, may hold values from 0 to 15, all different within a row; in each aligned block of 64 rows (0 to 63, 64 to 127, ...) at most 16 rows name the same one
- routed_expert_weight: float32 [2048, 2], P(('grp', 'ep', 'tp')), parts along dimension 0, may hold values from 0.1 to 1
- expert_gate_matrix: bfloat16 [16, 2048, 512], P(('ep', 'tp')), may hold values from -0.125 to 0.125
- expert_up_matrix: bfloat16 [16, 2048, 512], P(('ep', 'tp')), may hold values from -0.125 to 0.125
- expert_down_matrix: bfloat16 [16, 512, 2048], P(('ep', 'tp')), may hold values from -0.25 to 0.25
Outputs:
- mixer_out: bfloat16 [2048, 2048], P(('grp', 'ep', 'tp')), parts along dimension 0
- expert_out: bfloat16 [2048, 2048], P(('grp', 'ep', 'tp')), parts along dimension 0
There are 2 independent parts, one for each index of `grp`. A program takes and returns all parts, laid end to end along the dimension named above; an argument that names none is the same for every part. Nothing has to cross between parts.
Inputs may be any that keep to these rules, and one draw needn't show every extreme that they name: `routes`: each row names 2 different experts. In the rows of one device (aligned blocks of 64 rows) no expert is named more than 16 times, and in some blocks one expert is named exactly 16 times. `extra_log_forget`: mostly zero.
All inputs are finite; a program needn't handle non-finite values.
Results may differ from a plain program's by a relative error of at most 0.009.
Values may be sent and summed in bfloat16 or wider, within the bound.
A program may use at most 128 MiB of HBM per device.

v0:
```python
import jax
import jax.numpy as jnp
from jax import lax
from jax.sharding import PartitionSpec as P

lowest_log = -1e30
norm_eps = 1e-06
layer_eps = 1e-05


def prefix(value, axis, join, neutral, backward):
    count, mine = (lax.axis_size(axis), lax.axis_index(axis))
    pieces = jax.tree.map(lambda part: lax.all_gather(part, axis), value)
    if backward:
        pieces = jax.tree.map(lambda part: part[::-1], pieces)
        mine = count - 1 - mine
    so_far = jax.tree.map(
        lambda part, zero: jnp.full_like(part, 0) + jnp.asarray(zero, part.dtype), value, neutral
    )

    def lap(position, so_far):
        longer = join(so_far, jax.tree.map(lambda part: part[position], pieces))
        return jax.tree.map(lambda new, old: jnp.where(position < mine, new, old), longer, so_far)

    return lax.fori_loop(0, count - 1, lap, so_far)


def join_states(earlier, later):
    early_memory, early_top, early_total = earlier
    late_memory, late_top, late_total = later
    joined_top = jnp.maximum(late_total + early_top, late_top)
    joined_memory = (
        jnp.exp(late_total + early_top - joined_top) * early_memory
        + jnp.exp(late_top - joined_top) * late_memory
    )
    return (joined_memory, joined_top, early_total + late_total)


def block_summary(keys_f32, values_f32, log_weight):
    top_weight = jnp.max(log_weight)
    weighted = keys_f32 * jnp.exp(log_weight - top_weight)[:, None]
    memory = jnp.einsum("sd,se->de", weighted, values_f32, precision=lax.Precision.HIGHEST)
    return (memory, top_weight)


def block_output(
    queries,
    head_key_rows,
    head_value_rows,
    output_gate_logits,
    in_gate,
    through,
    before,
    span_total,
    prior_memory,
    prior_top,
    later_memory,
    later_top,
    head_norm_gain,
):
    score_scale = queries.shape[1] ** (-0.5)
    from_prior = through + prior_top
    from_later = span_total - before + later_top
    fw_log = through[:, None] - through[None, :] + in_gate[None, :]
    bw_log = before[None, :] - before[:, None] + in_gate[None, :]
    positions = jnp.arange(queries.shape[0])
    lower_mask = positions[:, None] >= positions[None, :]
    upper_mask = positions[:, None] <= positions[None, :]
    inner_top = jnp.maximum(
        jnp.max(jnp.where(lower_mask, fw_log, -jnp.inf), axis=1),
        jnp.max(jnp.where(upper_mask, bw_log, -jnp.inf), axis=1),
    )
    row_top = jnp.maximum(inner_top, jnp.maximum(from_prior, from_later))
    weights = jnp.where(lower_mask, jnp.exp(fw_log - row_top[:, None]), 0.0) + jnp.where(
        upper_mask, jnp.exp(bw_log - row_top[:, None]), 0.0
    )
    scores = (
        jnp.einsum("td,sd->ts", queries, head_key_rows, preferred_element_type=jnp.float32)
        * score_scale
    )
    near_weights = (scores * weights).astype(jnp.bfloat16)
    queries_f32 = queries.astype(jnp.float32)
    carried = jnp.exp(from_prior - row_top)[:, None] * jnp.dot(
        queries_f32, prior_memory, precision=lax.Precision.HIGHEST
    )
    carried = carried + jnp.exp(from_later - row_top)[:, None] * jnp.dot(
        queries_f32, later_memory, precision=lax.Precision.HIGHEST
    )
    head_rows = (
        jnp.dot(near_weights, head_value_rows, preferred_element_type=jnp.float32)
        + carried * score_scale
    )
    normed = (
        head_rows
        * lax.rsqrt(jnp.mean(head_rows * head_rows, axis=1, keepdims=True) + norm_eps)
        * head_norm_gain
    )
    return (jax.nn.sigmoid(output_gate_logits.astype(jnp.float32)) * normed).astype(jnp.bfloat16)


def mixer_part(
    queries,
    head_key_rows,
    head_value_rows,
    output_gate_logits,
    log_input_gate,
    forget_gate_logits,
    extra_log_forget,
    head_norm_gain,
    memory_output_matrix,
):
    forget_log_value = jax.nn.log_sigmoid(forget_gate_logits[0]) + extra_log_forget[0]
    in_gate = log_input_gate[0]
    through = jnp.cumsum(forget_log_value)
    before = through - forget_log_value
    span_total = through[-1]
    keys_f32 = head_key_rows.astype(jnp.float32)
    values_f32 = head_value_rows.astype(jnp.float32)
    fw_memory, fw_top = block_summary(keys_f32, values_f32, span_total - through + in_gate)
    bw_memory, bw_top = block_summary(keys_f32, values_f32, before + in_gate)
    identity = (
        jnp.zeros_like(fw_memory),
        jnp.array(lowest_log, jnp.float32),
        jnp.array(0.0, jnp.float32),
    )
    prior_memory, prior_top, _ = prefix(
        (fw_memory, fw_top, span_total), "ep", join_states, identity, False
    )
    later_memory, later_top, _ = prefix(
        (bw_memory, bw_top, span_total), "ep", join_states, identity, True
    )
    gated_rows = block_output(
        queries,
        head_key_rows,
        head_value_rows,
        output_gate_logits,
        in_gate,
        through,
        before,
        span_total,
        prior_memory,
        prior_top,
        later_memory,
        later_top,
        head_norm_gain,
    )
    return lax.psum_scatter(
        jnp.dot(gated_rows, memory_output_matrix, preferred_element_type=jnp.float32).astype(
            jnp.bfloat16
        ),
        "tp",
        scatter_dimension=0,
        tiled=True,
    )


def run_experts(arrived, expert_gate_matrix, expert_up_matrix, expert_down_matrix):
    gate_part = jnp.einsum(
        "nejd,edf->nejf", arrived, expert_gate_matrix, preferred_element_type=jnp.float32
    )
    up_part = jnp.einsum(
        "nejd,edf->nejf", arrived, expert_up_matrix, preferred_element_type=jnp.float32
    )
    hidden = (jax.nn.silu(gate_part) * up_part).astype(jnp.bfloat16)
    return jnp.einsum(
        "nejf,efd->nejd", hidden, expert_down_matrix, preferred_element_type=jnp.float32
    ).astype(jnp.bfloat16)


def expert_part(
    expert_input_tokens,
    expert_norm_gain,
    routes,
    routed_expert_weight,
    expert_gate_matrix,
    expert_up_matrix,
    expert_down_matrix,
):
    token_count, model_width = expert_input_tokens.shape
    top_count = routes.shape[1]
    local_experts = expert_gate_matrix.shape[0]
    ep_count = lax.axis_size("ep")
    tp_count = lax.axis_size("tp")
    devices = ep_count * tp_count
    expert_count = local_experts * devices
    capacity = max(2, 2 * token_count * top_count // expert_count)
    tokens_f32 = expert_input_tokens.astype(jnp.float32)
    centre = jnp.mean(tokens_f32, axis=1, keepdims=True)
    spread = jnp.mean(jnp.square(tokens_f32 - centre), axis=1, keepdims=True)
    normed = ((tokens_f32 - centre) * lax.rsqrt(spread + layer_eps) * expert_norm_gain).astype(
        jnp.bfloat16
    )
    flat_expert = routes.reshape(-1)
    one_hot = (flat_expert[:, None] == jnp.arange(expert_count, dtype=jnp.int32)[None, :]).astype(
        jnp.int32
    )
    earlier_count = jnp.cumsum(one_hot, axis=0) - one_hot
    slot_place = jnp.sum(earlier_count * one_hot, axis=1)
    slot_index = flat_expert * capacity + slot_place
    pair_row = jnp.arange(token_count * top_count, dtype=jnp.int32) // top_count
    source_row = jnp.zeros((expert_count * capacity,), jnp.int32).at[slot_index].set(pair_row)
    filled = jnp.zeros((expert_count * capacity,), jnp.int32).at[slot_index].set(1)
    outgoing = jnp.where(filled[:, None] > 0, normed[source_row], jnp.zeros((), jnp.bfloat16))
    sectioned = outgoing.reshape(ep_count, tp_count, local_experts * capacity, model_width)
    arrived = lax.all_to_all(
        lax.all_to_all(sectioned, "ep", split_axis=0, concat_axis=0, tiled=True),
        "tp",
        split_axis=1,
        concat_axis=1,
        tiled=True,
    )
    results = run_experts(
        arrived.reshape(devices, local_experts, capacity, model_width),
        expert_gate_matrix,
        expert_up_matrix,
        expert_down_matrix,
    )
    returned = lax.all_to_all(
        lax.all_to_all(
            results.reshape(ep_count, tp_count, local_experts * capacity, model_width),
            "ep",
            split_axis=0,
            concat_axis=0,
            tiled=True,
        ),
        "tp",
        split_axis=1,
        concat_axis=1,
        tiled=True,
    )
    returned = returned.reshape(expert_count * capacity, model_width)
    picked = returned[slot_index].reshape(token_count, top_count, model_width).astype(jnp.float32)
    combined = jnp.sum(routed_expert_weight[:, :, None] * picked, axis=1)
    return combined.astype(jnp.bfloat16)


def body(
    queries,
    head_key_rows,
    head_value_rows,
    output_gate_logits,
    log_input_gate,
    forget_gate_logits,
    extra_log_forget,
    head_norm_gain,
    memory_output_matrix,
    expert_input_tokens,
    expert_norm_gain,
    routes,
    routed_expert_weight,
    expert_gate_matrix,
    expert_up_matrix,
    expert_down_matrix,
):
    mixer_out = mixer_part(
        queries,
        head_key_rows,
        head_value_rows,
        output_gate_logits,
        log_input_gate,
        forget_gate_logits,
        extra_log_forget,
        head_norm_gain,
        memory_output_matrix,
    )
    expert_out = expert_part(
        expert_input_tokens,
        expert_norm_gain,
        routes,
        routed_expert_weight,
        expert_gate_matrix,
        expert_up_matrix,
        expert_down_matrix,
    )
    return (mixer_out, expert_out)


def solution(mesh):
    in_specs = (
        P(("grp", "ep"), "tp"),
        P(("grp", "ep"), "tp"),
        P(("grp", "ep"), "tp"),
        P(("grp", "ep"), "tp"),
        P("tp", ("grp", "ep")),
        P("tp", ("grp", "ep")),
        P("tp", ("grp", "ep")),
        P("tp"),
        P("tp", None),
        P(("grp", "ep", "tp"), None),
        P(),
        P(("grp", "ep", "tp"), None),
        P(("grp", "ep", "tp"), None),
        P(("ep", "tp"), None, None),
        P(("ep", "tp"), None, None),
        P(("ep", "tp"), None, None),
    )
    out_specs = (P(("grp", "ep", "tp"), None), P(("grp", "ep", "tp"), None))
    return jax.shard_map(body, mesh=mesh, in_specs=in_specs, out_specs=out_specs, check_vma=False)
```

profile of v0, /device:TPU:1, one launch (start us, length us, event | category | flops | bytes accessed | tf_op | source)
XLA Modules:
  0.0 208.9 jit_solution(7899996682373240851)
XLA Ops:
  9.3 1.4 fusion.81
  11.3 2.3 %fusion.40 = f32[256,512]{1,0:T(8,128)} fusion(bf16[256,512]{1,0:T(8,128)(2,1)} %param.22, bf16[256,256]{1,0:T(8,128)(2,1)} %param.21, f32[256]{0:T(256)S(1)} %subtract_exponential_fusion.2), kind=kOutput, calls=%fused_computation.48 | convolution fusion | flops 402784256 | bytes 918528 | tf_op jit(solution)/shard_map/sd,se->de/dot_general | solution.py:42
  22.2 5.5 %all-to-all-start = ((bf16[4,4,16,2048]{3,2,1,0:T(8,128)(2,1)}), bf16[4,4,16,2048]{3,2,1,0:T(8,128)(2,1)S(1)}, u32[]{:S(2)}, u32[]{:S(2)}) async-start(bf16[4,4,16,2048]{3,2,1,0:T(8,128)(2,1)} %broadcast_select_fusion), calls=%async_computation.1 | async-start | bytes 2097152 | tf_op jit(solution)/shard_map/all_to_all | solution.py:206
  33.9 46.7 %all-to-all-done = bf16[4,4,16,2048]{3,2,1,0:T(8,128)(2,1)S(1)} async-done(((bf16[4,4,16,2048]{3,2,1,0:T(8,128)(2,1)}), bf16[4,4,16,2048]{3,2,1,0:T(8,128)(2,1)S(1)}, u32[]{:S(2)}, u32[]{:S(2)}) %all-to-all-start) | async-done | bytes 1048608 | tf_op jit(solution)/shard_map/all_to_all | solution.py:206
  81.6 4.6 %all-to-all-start.1 = ((bf16[4,4,16,2048]{3,2,0,1:T(8,128)(2,1)}), bf16[4,4,16,2048]{3,2,0,1:T(8,128)(2,1)}, u32[]{:S(2)}, u32[]{:S(2)}) async-start(bf16[4,4,16,2048]{3,2,0,1:T(8,128)(2,1)} %copy.52), calls=%async_computation.2 | async-start | bytes 2097152 | tf_op jit(solution)/shard_map/all_to_all | solution.py:205
  86.3 1.4 dynamic-update-slice.1
  87.7 1.4 dynamic-update-slice.2
  89.1 8.3 %all-reduce.3 = (f32[4]{0:T(128)}, f32[4]{0:T(128)}, f32[4]{0:T(128)}) all-reduce(f32[4]{0:T(128)} %copy-done.15, f32[4]{0:T(128)S(1)} %dynamic-update-slice.1, f32[4]{0:T(128)S(1)} %dynamic-update-slice.2), channel_id=1, replica_groups=mesh['grp'=2,'ep'=4,'tp'=4] {'ep'}, use_global_device_ids=true, to_apply=%add | all-reduce | flops 12 | bytes 96
  102.0 1.5 copy.53
  104.4 1.5 fusion.7
  105.9 4.3 %convolution_convert_fusion = bf16[16,16,2048]{2,1,0:T(8,128)(2,1)} fusion(bf16[1,512,2048]{2,1,0:T(8,128)(2,1)S(1)} %copy-done, bf16[16,16,2048]{2,1,0:T(8,128)(2,1)} %bitcast.132, bf16[1,2048,512]{2,1,0:T(8,128)(2,1)} %param.34, f32[16,1,16,512]{3,2,0,1:T(8,128)} %fusion.7), kind=kOutput, calls=%fused_computation.8 | convolution fusion | flops 1075052544 | bytes 6815744 | tf_op jit(solution)/shard_map/nejf,efd->nejd/dot_general | solution.py:165
  110.3 4.2 %all-to-all-start.2 = ((bf16[4,4,16,2048]{3,2,1,0:T(8,128)(2,1)}), bf16[4,4,16,2048]{3,2,1,0:T(8,128)(2,1)}, u32[]{:S(2)}, u32[]{:S(2)}) async-start(bf16[4,4,16,2048]{3,2,1,0:T(8,128)(2,1)} %bitcast.130), calls=%async_computation.3 | async-start | bytes 2097152 | tf_op jit(solution)/shard_map/all_to_all | solution.py:219
  114.6 3.2 %rev.11 = f32[4,256,512]{2,1,0:T(8,128)} reverse(f32[4,256,512]{2,1,0:T(8,128)} %bitcast.129), dimensions={0} | reverse | bytes 4194304 | tf_op jit(solution)/shard_map/rev | solution.py:15
  117.7 16.7 %while.33 = (s32[]{:T(128)}, f32[256,512]{1,0:T(8,128)S(1)}, f32[]{:T(128)}, s32[]{:T(128)}, f32[4]{0:T(128)}, /*index=5*/f32[4]{0:T(128)}, f32[4,256,512]{2,1,0:T(8,128)}, s32[]{:T(128)}, s32[]{:T(128)}) while((s32[]{:T(128)}, f32[256,512]{1,0:T(8,128)S(1)}, f32[]{:T(128)}, s32[]{:T(128)}, f32[4]{0:T(128)}, ...), condition=%wide.region_9.10_spmd.clone, body=%wide.region_8.9_spmd.clone.sunk | while | flops 655369 | bytes 1573090 | solution.py:25
  121.8 1.5 fusion.99
  127.4 1.5 fusion.99
  133.0 1.5 fusion.99
  134.4 6.4 %all-gather.5.cloned.1.call-done = f32[1024,512]{1,0:T(8,128)} async-done(((f32[256,512]{1,0:T(8,128)}), f32[1024,512]{1,0:T(8,128)}) %all-gather.5.cloned.1.call-update) | async-done | bytes 2097168 | tf_op jit(solution)/shard_map/all_gather | solution.py:13
  140.8 17.5 %while.32 = (s32[]{:T(128)}, f32[256,512]{1,0:T(8,128)S(1)}, f32[]{:T(128)}, s32[]{:T(128)}, f32[4]{0:T(128)}, /*index=5*/f32[4]{0:T(128)}, f32[4,256,512]{2,1,0:T(8,128)}, s32[]{:T(128)}, s32[]{:T(128)}) while((s32[]{:T(128)}, f32[256,512]{1,0:T(8,128)S(1)}, f32[]{:T(128)}, s32[]{:T(128)}, f32[4]{0:T(128)}, ...), condition=%wide.region_6.7_spmd.clone, body=%wide.region_5.6_spmd.clone.sunk | while | flops 655369 | bytes 1573090 | solution.py:25
  145.2 1.5 fusion.98
  151.1 1.5 fusion.98
  156.9 1.5 fusion.98
  160.2 1.4 convolution_multiply_fusion.1
  161.5 1.4 fusion.18
  163.0 2.2 %multiply_reduce_fusion.1 = (f32[256]{0:T(256)S(1)}, f32[256,512]{1,0:T(8,128)}) fusion(f32[256,512]{1,0:T(8,128)S(1)} %fusion.18, bf16[256,512]{1,0:T(8,128)(2,1)S(1)} %copy-done.3, bf16[256,256]{1,0:T(8,128)(2,1)} %param.20, bf16[256,256]{1,0:T(8,128)(2,1)S(1)} %copy-done.4, f32[256]{0:T(256)S(1)} %copy-done.9, f32[256]{0:T(256)S(1)} %get-tuple-element.341, ...), kind=kOutput, calls=%fused_computation.44 | convolution fusion | flops 101973760 | bytes 1579008 | tf_op jit(solution)/shard_map/dot_general | solution.py:90
  165.1 3.7 %convolution_convert_fusion.1 = bf16[256,2048]{1,0:T(8,128)(2,1)} fusion(bf16[512,2048]{1,0:T(8,128)(2,1)} %param.28, f32[256,512]{1,0:T(8,128)} %get-tuple-element.346, bf16[256,512]{1,0:T(8,128)(2,1)} %param.23, f32[512]{0:T(512)} %param.27, f32[256]{0:T(256)S(1)} %add_rsqrt_fusion), kind=kOutput, calls=%fused_computation.9 | convolution fusion | flops 538443776 | bytes 3935232 | tf_op jit(solution)/shard_map/dot_general | solution.py:148
  168.9 2.4 %copy.54 = bf16[4,4,16,2048]{3,2,0,1:T(8,128)(2,1)} copy(bf16[4,4,16,2048]{3,2,1,0:T(8,128)(2,1)} %all-to-all-done.2) | data formatting | bytes 2097152 | tf_op jit(solution)/shard_map/all_to_all | solution.py:219
  171.2 6.3 %all-to-all-start.3 = ((bf16[4,4,16,2048]{3,2,0,1:T(8,128)(2,1)}), bf16[4,4,16,2048]{3,2,0,1:T(8,128)(2,1)}, u32[]{:S(2)}, u32[]{:S(2)}) async-start(bf16[4,4,16,2048]{3,2,0,1:T(8,128)(2,1)} %copy.54), calls=%async_computation.4 | async-start | bytes 2097152 | tf_op jit(solution)/shard_map/all_to_all | solution.py:218
  177.6 17.7 %all-to-all-done.3 = bf16[4,4,16,2048]{3,2,0,1:T(8,128)(2,1)} async-done(((bf16[4,4,16,2048]{3,2,0,1:T(8,128)(2,1)}), bf16[4,4,16,2048]{3,2,0,1:T(8,128)(2,1)}, u32[]{:S(2)}, u32[]{:S(2)}) %all-to-all-start.3) | async-done | bytes 1048608 | tf_op jit(solution)/shard_map/all_to_all | solution.py:218
  196.6 1.7 gather_fusion.1
  198.4 1.7 reshape.281
  200.1 2.2 %multiply_reduce_fusion = bf16[64,2048]{1,0:T(8,128)(2,1)} fusion(f32[64,2,2048]{2,1,0:T(2,128)S(1)} %reshape.281, f32[64,2]{1,0:T(8,128)S(1)} %copy.49), kind=kLoop, calls=%fused_computation.29 | loop fusion | flops 393216 | bytes 1311232 | tf_op jit(solution)/shard_map/reduce_sum | solution.py:233
  (108 shorter events, 41.6 us)
Async XLA Ops:
  7.2 98.8 %copy-start = (bf16[1,512,2048]{2,1,0:T(8,128)(2,1)S(1)}, bf16[1,512,2048]{2,1,0:T(8,128)(2,1)}, u32[]{:S(2)}) copy-start(bf16[1,512,2048]{2,1,0:T(8,128)(2,1)} %param.35) | copy-start | bytes 6291460
  7.2 12.0 %copy-start.1 = (bf16[64,2048]{1,0:T(8,128)(2,1)S(1)}, bf16[64,2048]{1,0:T(8,128)(2,1)}, u32[]{:S(2)}) copy-start(bf16[64,2048]{1,0:T(8,128)(2,1)} %param.29) | copy-start | bytes 786436
  7.2 12.3 %copy-start.7 = (f32[2048]{0:T(1024)S(1)}, f32[2048]{0:T(1024)}, u32[]{:S(2)}) copy-start(f32[2048]{0:T(1024)} %param.30) | copy-start | bytes 24580
  7.2 107.4 %all-gather.7.cloned.1.call-start = ((), (), s32[]{:S(2)}) async-start(), calls=%async_computation.7 | async-start | bytes 2621440 | tf_op jit(solution)/shard_map/all_gather | solution.py:13
  16.0 5.0 %copy-start.12 = (s32[128]{0:T(128)}, s32[128]{0:T(128)S(1)}, u32[]{:S(2)}) copy-start(s32[128]{0:T(128)S(1)} %fusion.71) | copy-start | bytes 1540
  21.0 9.1 %copy-start.5 = (f32[1,256]{1,0:T(1,128)S(1)}, f32[1,256]{1,0:T(1,128)}, u32[]{:S(2)}) copy-start(f32[1,256]{1,0:T(1,128)} %param.24) | copy-start | bytes 3076
  21.0 11.5 %copy-start.3 = (bf16[256,512]{1,0:T(8,128)(2,1)S(1)}, bf16[256,512]{1,0:T(8,128)(2,1)}, u32[]{:S(2)}) copy-start(bf16[256,512]{1,0:T(8,128)(2,1)} %param.22) | copy-start | bytes 786436
  21.0 11.5 %copy-start.4 = (bf16[256,256]{1,0:T(8,128)(2,1)S(1)}, bf16[256,256]{1,0:T(8,128)(2,1)}, u32[]{:S(2)}) copy-start(bf16[256,256]{1,0:T(8,128)(2,1)} %param.21) | copy-start | bytes 393220
  22.2 5.5 %copy-start.16 = (u32[32]{0:T(128)S(1)}, u32[32]{0:T(128)}, u32[]{:S(2)}) copy-start(u32[32]{0:T(128)} %constant.123) | copy-start | bytes 388
  22.2 58.4 %all-to-all-start = ((bf16[4,4,16,2048]{3,2,1,0:T(8,128)(2,1)}), bf16[4,4,16,2048]{3,2,1,0:T(8,128)(2,1)S(1)}, u32[]{:S(2)}, u32[]{:S(2)}) async-start(bf16[4,4,16,2048]{3,2,1,0:T(8,128)(2,1)} %broadcast_select_fusion), calls=%async_computation.1 | async-start | bytes 2097152 | tf_op jit(solution)/shard_map/all_to_all | solution.py:206
  27.7 113.1 %all-gather.5.cloned.1.call-start = ((), (), s32[]{:S(2)}) async-start(), calls=%async_computation.6 | async-start | bytes 2621440 | tf_op jit(solution)/shard_map/all_gather | solution.py:13
  29.5 0.5 copy-start.15
  33.9 66.0 %copy-start.6 = (f32[1,256]{1,0:T(1,128)S(1)}, f32[1,256]{1,0:T(1,128)}, u32[]{:S(2)}) copy-start(f32[1,256]{1,0:T(1,128)} %param.26) | copy-start | bytes 3076
  81.6 20.3 %all-to-all-start.1 = ((bf16[4,4,16,2048]{3,2,0,1:T(8,128)(2,1)}), bf16[4,4,16,2048]{3,2,0,1:T(8,128)(2,1)}, u32[]{:S(2)}, u32[]{:S(2)}) async-start(bf16[4,4,16,2048]{3,2,0,1:T(8,128)(2,1)} %copy.52), calls=%async_computation.2 | async-start | bytes 2097152 | tf_op jit(solution)/shard_map/all_to_all | solution.py:205
  100.6 0.6 copy-start.10
  102.0 2.5 %copy-start.14 = (bf16[1,2048,512]{2,1,0:T(8,128)(2,1)S(1)}, bf16[1,2048,512]{2,1,0:T(8,128)(2,1)}, u32[]{:S(2)}) copy-start(bf16[1,2048,512]{2,1,0:T(8,128)(2,1)} %param.33) | copy-start | bytes 6291460
  103.4 1.0 copy-start.2
  110.3 58.6 %all-to-all-start.2 = ((bf16[4,4,16,2048]{3,2,1,0:T(8,128)(2,1)}), bf16[4,4,16,2048]{3,2,1,0:T(8,128)(2,1)}, u32[]{:S(2)}, u32[]{:S(2)}) async-start(bf16[4,4,16,2048]{3,2,1,0:T(8,128)(2,1)} %bitcast.130), calls=%async_computation.3 | async-start | bytes 2097152 | tf_op jit(solution)/shard_map/all_to_all | solution.py:219
  114.5 87.8 %reduce-scatter.2.cloned.1.call-start = ((), (), s32[]{:S(2)}) async-start(), calls=%async_computation.5 | async-start | bytes 1310720 | tf_op jit(solution)/shard_map/reduce_scatter | solution.py:147
  159.6 0.6 copy-start.8
  160.2 2.8 %copy-start.9 = (f32[256]{0:T(256)S(1)}, f32[256]{0:T(256)}, u32[]{:S(2)}) copy-start(f32[256]{0:T(256)} %copy-done.8) | copy-start | bytes 3076
  168.8 8.7 %copy-start.11 = (f32[64,2]{0,1:T(2,128)S(1)}, f32[64,2]{0,1:T(2,128)}, u32[]{:S(2)}) copy-start(f32[64,2]{0,1:T(2,128)} %param.32) | copy-start | bytes 1540
  168.8 8.8 %copy-start.13 = (s32[128]{0:T(128)S(1)}, s32[128]{0:T(128)}, u32[]{:S(2)}) copy-start(s32[128]{0:T(128)} %copy-done.12) | copy-start | bytes 1540
  171.2 24.1 %all-to-all-start.3 = ((bf16[4,4,16,2048]{3,2,0,1:T(8,128)(2,1)}), bf16[4,4,16,2048]{3,2,0,1:T(8,128)(2,1)}, u32[]{:S(2)}, u32[]{:S(2)}) async-start(bf16[4,4,16,2048]{3,2,0,1:T(8,128)(2,1)} %copy.54), calls=%async_computation.4 | async-start | bytes 2097152 | tf_op jit(solution)/shard_map/all_to_all | solution.py:218
Sparse Core Ops, SparseCore 0:
  13.8 70.0 all-gather.6
  85.4 55.3 all-gather.4
  168.9 29.0 reduce-scatter.1
where the time goes:
time: 212 us; the launch traced here: 209 us
  waiting for transfers between devices  70.9 us (33%)
  local copies, waits for them, and re-layouts  41.9 us (20%)
  other arithmetic  23.9 us (11%)
  starting transfers between devices  20.8 us (10%)
  matrix products  18 us (8%)
  between operations  14.1 us (7%)
  loops' own time  11.1 us (5%)
  blocking collectives  8.26 us (4%)
    all_to_all x1, waiting for transfers between devices, expert_part(): lax.all_to_all(sectioned, 'ep', split_axis=0, concat_axis=0, tiled=True)  46.7 us
    all_to_all x1, waiting for transfers between devices, expert_part(): lax.all_to_all(lax.all_to_all(results.reshape(ep_count, tp_count, local_e...  17.7 us
    dynamic_slice x12, local copies, waits for them, and re-layouts, lap(): longer = join(so_far, jax.tree.map(lambda part: part[position], pieces))  14.4 us
    another operation x2, loops' own time, prefix(): return lax.fori_loop(0, count - 1, lap, so_far)  11.1 us
    select_n x6, other arithmetic, lap(): jnp.where(position < mine, new, old)  8.71 us
    unnamed x1, blocking collectives  8.26 us
    unnamed x42, local copies, waits for them, and re-layouts  6.98 us
    all_gather x2, waiting for transfers between devices, prefix(): pieces = jax.tree.map(lambda part: lax.all_gather(part, axis), value)  6.44 us
  transfers between devices with their start and end apart: 7, of which 3 were waited for; matrix products, arithmetic and copies ran while one was open for 36% of the time, Pallas kernels for 0%

commit v1 on v0

v1 whole, which is shorter than its diff:
```python
import functools

import jax
import jax.numpy as jnp
from jax import lax
from jax.experimental import pallas as pl
from jax.experimental.pallas import tpu as pltpu
from jax.sharding import PartitionSpec as P

lowest_log = -1e30
norm_eps = 1e-06
layer_eps = 1e-05
row_tile = 16

F32 = jnp.float32
BF16 = jnp.bfloat16


def dot(a, b, contract=((1,), (0,))):
    return lax.dot_general(a, b, (contract, ((), ())), preferred_element_type=F32)


def step_kernel(
    ep,
    tp,
    stride,
    capacity,
    q_ref,
    k_ref,
    v_ref,
    og_ref,
    ig_ref,
    fg_ref,
    xf_ref,
    hgain_ref,
    wo_hbm,
    tok_ref,
    egain_ref,
    routes_ref,
    rw_ref,
    wg_hbm,
    wu_hbm,
    wd_hbm,
    mix_ref,
    exp_ref,
    wo,
    wg,
    wu,
    wd,
    out_rows,
    arrived,
    results,
    returned,
    comb,
    fw_own,
    bw_own,
    fw_in,
    bw_in,
    fw_out,
    bw_out,
    fw_top_in,
    bw_top_in,
    fw_top_out,
    bw_top_out,
    parts_out,
    parts_in,
    gated,
    hidden,
    w_sem,
    d_send,
    d_recv,
    r_send,
    r_recv,
    c_send,
    c_recv,
    p_send,
    p_recv,
):
    n = ep * tp
    z = lax.axis_index("ep")
    t = lax.axis_index("tp")
    me = z * tp + t
    span = q_ref.shape[0]
    tokens, width = tok_ref.shape
    sub = span // tp

    def peer(dz, dt):
        return lax.rem(z + dz, ep), lax.rem(t + dt, tp)

    def to(z2, t2):
        return {"ep": z2, "tp": t2}

    barrier = pltpu.get_barrier_semaphore()

    def greet(i, c):
        z2, t2 = peer(i // tp, lax.rem(i, tp))
        pl.semaphore_signal(
            barrier, inc=1, device_id=to(z2, t2), device_id_type=pl.DeviceIdType.MESH
        )
        return c

    lax.fori_loop(1, n, greet, 0)

    loads = [
        pltpu.make_async_copy(src, dst, w_sem.at[i])
        for i, (src, dst) in enumerate(
            ((wo_hbm, wo), (wg_hbm.at[0], wg), (wu_hbm.at[0], wu), (wd_hbm.at[0], wd))
        )
    ]
    for load in loads:
        load.start()

    rows_i = lax.broadcasted_iota(jnp.int32, (span, span), 0)
    cols_i = lax.broadcasted_iota(jnp.int32, (span, span), 1)
    lower = rows_i >= cols_i
    upper = rows_i <= cols_i
    diag = rows_i == cols_i

    fg = fg_ref[...]
    lf_row = jnp.minimum(fg, 0.0) - jnp.log1p(jnp.exp(-jnp.abs(fg))) + xf_ref[...]
    in_row = ig_ref[...]
    lf_col = jnp.sum(jnp.where(diag, lf_row, 0.0), axis=1, keepdims=True)
    in_col = jnp.sum(jnp.where(diag, in_row, 0.0), axis=1, keepdims=True)
    through_col = jnp.sum(jnp.where(lower, lf_row, 0.0), axis=1, keepdims=True)
    through_row = jnp.sum(jnp.where(upper, lf_col, 0.0), axis=0, keepdims=True)
    before_col = through_col - lf_col
    before_row = through_row - lf_row
    total = jnp.sum(lf_row, axis=1, keepdims=True)

    keys = k_ref[...]
    values = v_ref[...]
    keys_f32 = keys.astype(F32)
    fw_w = total - through_col + in_col
    bw_w = before_col + in_col
    fw_top = jnp.max(fw_w, axis=0, keepdims=True)
    bw_top = jnp.max(bw_w, axis=0, keepdims=True)
    fw_own[...] = dot((keys_f32 * jnp.exp(fw_w - fw_top)).astype(BF16), values, ((0,), (0,)))
    bw_own[...] = dot((keys_f32 * jnp.exp(bw_w - bw_top)).astype(BF16), values, ((0,), (0,)))

    x = tok_ref[...].astype(F32)
    centre = jnp.mean(x, axis=1, keepdims=True)
    spread = jnp.mean(jnp.square(x - centre), axis=1, keepdims=True)
    normed = ((x - centre) * lax.rsqrt(spread + layer_eps) * egain_ref[...]).astype(BF16)
    routes = routes_ref[...]
    lanes = max(128, -(-n // 128) * 128)
    lane_e = lax.broadcasted_iota(jnp.int32, (tokens, lanes), 1)
    top = routes.shape[1]
    hots = [(lane_e == routes[:, i : i + 1]).astype(F32) for i in range(top)]
    tok_r = lax.broadcasted_iota(jnp.int32, (tokens, tokens), 0)
    tok_c = lax.broadcasted_iota(jnp.int32, (tokens, tokens), 1)
    earlier = dot((tok_r > tok_c).astype(F32).astype(BF16), sum(hots).astype(BF16))
    slot_i = lax.broadcasted_iota(jnp.int32, (tokens, n * stride), 1)
    pick = jnp.zeros((tokens, n * stride), F32)
    weigh = jnp.zeros((tokens, n * stride), F32)
    for i in range(top):
        place = jnp.sum(earlier * hots[i], axis=1, keepdims=True).astype(jnp.int32)
        mine = (slot_i == routes[:, i : i + 1] * stride + place).astype(F32)
        pick = pick + mine
        weigh = weigh + mine * rw_ref[:, i : i + 1]
    comb[...] = weigh
    pick = pick.astype(BF16)
    out_rows[...] = dot(pick, normed, ((0,), (0,))).astype(BF16)

    pl.semaphore_wait(barrier, n - 1)

    def rows_of(ref, index):
        return ref.at[pl.ds(pl.multiple_of(index * stride, row_tile), stride)]

    def exchange(src, dst, send, recv, z2, t2, arriving):
        p = z2 * tp + t2
        return pltpu.make_async_remote_copy(
            src_ref=rows_of(src, p),
            dst_ref=rows_of(dst, p if arriving else me),
            send_sem=send.at[p],
            recv_sem=recv.at[p if arriving else me],
            device_id=to(z2, t2),
            device_id_type=pl.DeviceIdType.MESH,
        )

    def dispatch(z2, t2, arriving=False):
        return exchange(out_rows, arrived, d_send, d_recv, z2, t2, arriving)

    def give_back(z2, t2, arriving=False):
        return exchange(results, returned, r_send, r_recv, z2, t2, arriving)

    def each_peer(first, action):
        def turn(i, c):
            z2, t2 = peer(i // tp, lax.rem(i, tp))
            action(z2, t2)
            return c

        lax.fori_loop(first, n, turn, 0)

    own = pl.ds(pl.multiple_of(me * stride, row_tile), stride)

    def chain(index, src, dst, z2):
        return pltpu.make_async_remote_copy(
            src_ref=src,
            dst_ref=dst,
            send_sem=c_send.at[index],
            recv_sem=c_recv.at[index],
            device_id=to(z2, t),
            device_id_type=pl.DeviceIdType.MESH,
        )

    after = lax.rem(z + 1, ep)
    ahead = lax.rem(z + ep - 1, ep)
    fw_chain = (chain(0, fw_top_out, fw_top_in, after), chain(1, fw_out, fw_in, after))
    bw_chain = (chain(2, bw_top_out, bw_top_in, ahead), chain(3, bw_out, bw_in, ahead))

    @pl.when(z == 0)
    def _():
        fw_in[...] = jnp.zeros_like(fw_in)
        fw_top_in[...] = jnp.full_like(fw_top_in, lowest_log)

    @pl.when(z == ep - 1)
    def _():
        bw_in[...] = jnp.zeros_like(bw_in)
        bw_top_in[...] = jnp.full_like(bw_top_in, lowest_log)

    def pass_on(copies, in_ref, top_in, own_ref, own_top, out_ref, top_out):
        shifted = total + top_in[0:1, 0:1]
        joined = jnp.maximum(shifted, own_top)
        out_ref[...] = (
            jnp.exp(shifted - joined) * in_ref[...].astype(F32)
            + jnp.exp(own_top - joined) * own_ref[...]
        ).astype(BF16)
        top_out[...] = jnp.broadcast_to(joined, top_out.shape)
        for copy in copies:
            copy.start()

    def stage(s, c):
        @pl.when(z == s)
        def _():
            @pl.when(z > 0)
            def _():
                for copy in fw_chain:
                    copy.wait_recv()

            pass_on(fw_chain, fw_in, fw_top_in, fw_own, fw_top, fw_out, fw_top_out)

        @pl.when(ep - 1 - z == s)
        def _():
            @pl.when(z < ep - 1)
            def _():
                for copy in bw_chain:
                    copy.wait_recv()

            pass_on(bw_chain, bw_in, bw_top_in, bw_own, bw_top, bw_out, bw_top_out)

        def plane(dt, c2):
            z2, t2 = peer(s + 1, dt)
            dispatch(z2, t2).start()
            return c2

        return lax.fori_loop(0, tp, plane, c)

    def near_plane(dt, c):
        z2, t2 = peer(0, dt)
        dispatch(z2, t2).start()
        return c

    lax.fori_loop(1, tp, near_plane, 0)
    lax.fori_loop(0, ep - 1, stage, 0)
    arrived[own] = out_rows[own]

    from_row = through_col - through_row + in_row
    fw_log = jnp.where(lower, from_row, -jnp.inf)
    bw_log = jnp.where(upper, before_row - before_col + in_row, -jnp.inf)
    inner_top = jnp.maximum(
        jnp.max(fw_log, axis=1, keepdims=True), jnp.max(bw_log, axis=1, keepdims=True)
    )

    @pl.when(z == ep - 1)
    def _():
        for copy in fw_chain:
            copy.wait_recv()

    @pl.when(z == 0)
    def _():
        for copy in bw_chain:
            copy.wait_recv()

    from_prior = through_col + fw_top_in[0:1, 0:1]
    from_later = total - before_col + bw_top_in[0:1, 0:1]
    row_top = jnp.maximum(inner_top, jnp.maximum(from_prior, from_later))
    weights = jnp.exp(fw_log - row_top) + jnp.exp(bw_log - row_top)
    queries = q_ref[...]
    scale = queries.shape[1] ** (-0.5)
    scores = dot(queries, keys, ((1,), (1,))) * scale
    near = (scores * weights).astype(BF16)
    carried = jnp.exp(from_prior - row_top) * dot(queries, fw_in[...])
    carried = carried + jnp.exp(from_later - row_top) * dot(queries, bw_in[...])
    head_rows = dot(near, values) + carried * scale
    mean_square = jnp.mean(head_rows * head_rows, axis=1, keepdims=True)
    normed_rows = head_rows * lax.rsqrt(mean_square + norm_eps) * hgain_ref[...]
    gated[...] = (jax.nn.sigmoid(og_ref[...].astype(F32)) * normed_rows).astype(BF16)

    loads[0].wait()
    cols = 256

    def project(i, c):
        at = pl.ds(pl.multiple_of(i * cols, cols), cols)
        parts_out[:, at] = dot(gated[...], wo[:, at]).astype(BF16)
        return c

    lax.fori_loop(0, width // cols, project, 0)

    def share(dt, arriving=False):
        t2 = lax.rem(t + dt, tp)
        slot = t2 if arriving else t
        return pltpu.make_async_remote_copy(
            src_ref=parts_out.at[pl.ds(pl.multiple_of(t2 * sub, row_tile), sub)],
            dst_ref=parts_in.at[slot],
            send_sem=p_send.at[t2],
            recv_sem=p_recv.at[slot],
            device_id=to(z, t2),
            device_id_type=pl.DeviceIdType.MESH,
        )

    for dt in range(1, tp):
        share(dt).start()
    parts_in[t] = parts_out[pl.ds(pl.multiple_of(t * sub, row_tile), sub), :]

    for load in loads[1:]:
        load.wait()
    each_peer(1, lambda z2, t2: dispatch(z2, t2, True).wait_recv())
    fe = wg.shape[1]
    chunk = min(256, n * stride)

    def expert_chunk(i, c):
        at = pl.ds(pl.multiple_of(i * chunk, chunk), chunk)

        def up(j, c2):
            f = pl.ds(pl.multiple_of(j * cols, cols), cols)
            rows = arrived[at, :]
            gate_part = dot(rows, wg[:, f])
            up_part = dot(rows, wu[:, f])
            hidden[:, f] = (gate_part * jax.nn.sigmoid(gate_part) * up_part).astype(BF16)
            return c2

        lax.fori_loop(0, fe // cols, up, 0)

        def down(j, c2):
            f = pl.ds(pl.multiple_of(j * cols, cols), cols)
            results[at, f] = dot(hidden[...], wd[:, f]).astype(BF16)
            return c2

        return lax.fori_loop(0, width // cols, down, c)

    lax.fori_loop(0, n * stride // chunk, expert_chunk, 0)
    each_peer(1, lambda z2, t2: give_back(z2, t2).start())
    returned[own] = results[own]

    for dt in range(1, tp):
        share(dt, True).wait_recv()
    mixed = parts_in[0].astype(F32)
    for i in range(1, tp):
        mixed = mixed + parts_in[i].astype(F32)
    mix_ref[...] = mixed.astype(BF16)

    weigh = comb[...]
    high = weigh.astype(BF16)
    low = (weigh - high.astype(F32)).astype(BF16)
    each_peer(1, lambda z2, t2: give_back(z2, t2, True).wait_recv())
    for j in range(width // cols):
        f = slice(j * cols, (j + 1) * cols)
        rows = returned[:, f]
        exp_ref[:, f] = (dot(high, rows) + dot(low, rows)).astype(BF16)

    @pl.when(z < ep - 1)
    def _():
        for copy in fw_chain:
            copy.wait_send()

    @pl.when(z > 0)
    def _():
        for copy in bw_chain:
            copy.wait_send()

    for dt in range(1, tp):
        share(dt).wait_send()
    each_peer(1, lambda z2, t2: dispatch(z2, t2).wait_send())
    each_peer(1, lambda z2, t2: give_back(z2, t2).wait_send())


def body(
    queries,
    head_key_rows,
    head_value_rows,
    output_gate_logits,
    log_input_gate,
    forget_gate_logits,
    extra_log_forget,
    head_norm_gain,
    memory_output_matrix,
    expert_input_tokens,
    expert_norm_gain,
    routes,
    routed_expert_weight,
    expert_gate_matrix,
    expert_up_matrix,
    expert_down_matrix,
):
    ep = lax.axis_size("ep")
    tp = lax.axis_size("tp")
    n = ep * tp
    span, dqk = queries.shape
    dv = head_value_rows.shape[1]
    tokens, width = expert_input_tokens.shape
    fe = expert_gate_matrix.shape[2]
    capacity = max(2, 2 * tokens * routes.shape[1] // n)
    stride = -(-capacity // row_tile) * row_tile
    slots = n * stride
    vmem = pl.BlockSpec(memory_space=pltpu.VMEM)
    hbm = pl.BlockSpec(memory_space=pl.ANY)
    dma = pltpu.SemaphoreType.DMA
    return pl.pallas_call(
        functools.partial(step_kernel, ep, tp, stride, capacity),
        out_shape=(
            jax.ShapeDtypeStruct((span // tp, width), BF16),
            jax.ShapeDtypeStruct((tokens, width), BF16),
        ),
        in_specs=[vmem] * 8 + [hbm] + [vmem] * 4 + [hbm] * 3,
        out_specs=(vmem, vmem),
        scratch_shapes=[
            pltpu.VMEM((dv, width), BF16),
            pltpu.VMEM((width, fe), BF16),
            pltpu.VMEM((width, fe), BF16),
            pltpu.VMEM((fe, width), BF16),
            pltpu.VMEM((slots, width), BF16),
            pltpu.VMEM((slots, width), BF16),
            pltpu.VMEM((slots, width), BF16),
            pltpu.VMEM((slots, width), BF16),
            pltpu.VMEM((tokens, slots), F32),
            pltpu.VMEM((dqk, dv), F32),
            pltpu.VMEM((dqk, dv), F32),
            pltpu.VMEM((dqk, dv), BF16),
            pltpu.VMEM((dqk, dv), BF16),
            pltpu.VMEM((dqk, dv), BF16),
            pltpu.VMEM((dqk, dv), BF16),
            pltpu.VMEM((8, 128), F32),
            pltpu.VMEM((8, 128), F32),
            pltpu.VMEM((8, 128), F32),
            pltpu.VMEM((8, 128), F32),
            pltpu.VMEM((span, width), BF16),
            pltpu.VMEM((tp, span // tp, width), BF16),
            pltpu.VMEM((span, dv), BF16),
            pltpu.VMEM((min(256, slots), fe), BF16),
            dma((4,)),
            dma((n,)),
            dma((n,)),
            dma((n,)),
            dma((n,)),
            dma((4,)),
            dma((4,)),
            dma((tp,)),
            dma((tp,)),
        ],
        compiler_params=pltpu.CompilerParams(
            collective_id=0, has_side_effects=True, vmem_limit_bytes=64 * 1024 * 1024 - 65536
        ),
    )(
        queries,
        head_key_rows,
        head_value_rows,
        output_gate_logits,
        log_input_gate,
        forget_gate_logits,
        extra_log_forget,
        head_norm_gain[None, :],
        memory_output_matrix,
        expert_input_tokens,
        expert_norm_gain[None, :],
        routes,
        routed_expert_weight,
        expert_gate_matrix,
        expert_up_matrix,
        expert_down_matrix,
    )


def solution(mesh):
    in_specs = (
        P(("grp", "ep"), "tp"),
        P(("grp", "ep"), "tp"),
        P(("grp", "ep"), "tp"),
        P(("grp", "ep"), "tp"),
        P("tp", ("grp", "ep")),
        P("tp", ("grp", "ep")),
        P("tp", ("grp", "ep")),
        P("tp"),
        P("tp", None),
        P(("grp", "ep", "tp"), None),
        P(),
        P(("grp", "ep", "tp"), None),
        P(("grp", "ep", "tp"), None),
        P(("ep", "tp"), None, None),
        P(("ep", "tp"), None, None),
        P(("ep", "tp"), None, None),
    )
    out_specs = (P(("grp", "ep", "tp"), None), P(("grp", "ep", "tp"), None))
    return jax.shard_map(body, mesh=mesh, in_specs=in_specs, out_specs=out_specs, check_vma=False)
```

time: 212 us -> 89.6 us (0.42); the launches traced: 209 us -> 88.6 us
  Pallas kernels: 0 us -> 81.9 us
  waiting for transfers between devices: 70.9 us -> 0 us
  local copies, waits for them, and re-layouts: 41.9 us -> 6.1 us
  other arithmetic: 23.9 us -> 0 us
  starting transfers between devices: 20.8 us -> 0 us
  matrix products: 18 us -> 0 us
  between operations: 14.1 us -> 0.64 us
  loops' own time: 11.1 us -> 0 us
  blocking collectives: 8.26 us -> 0 us
    pallas_call x0 -> x1, Pallas kernels: none -> 81.9 us  [body(): pl.pallas_call(functools.partial(step_kernel, ep, tp, stride, capacity),...]
    all_to_all x4 -> x0, waiting for transfers between devices: 64.4 us -> none  [the longest x1 46.7 us: expert_part(): lax.all_to_all(sectioned, 'ep', split_axis=0, concat_axis=0, tiled=True)]
    all_to_all x4 -> x0, starting transfers between devices: 20.7 us -> none  [the longest x1 6.27 us: expert_part(): lax.all_to_all(lax.all_to_all(results.reshape(ep_count, tp_count, local_e...]
    dot_general x8 -> x0, matrix products: 18 us -> none  [the longest x1 4.33 us: run_experts(): jnp.einsum('nejf,efd->nejd', hidden, expert_down_matrix, preferred_elemen...]
    dynamic_slice x12 -> x0, local copies, waits for them, and re-layouts: 14.4 us -> none  [lap(): longer = join(so_far, jax.tree.map(lambda part: part[position], pieces))]
    another operation x2 -> x0, loops' own time: 11.1 us -> none  [prefix(): return lax.fori_loop(0, count - 1, lap, so_far)]
    select_n x10 -> x0, other arithmetic: 9.85 us -> none  [the longest x6 8.71 us: lap(): jnp.where(position < mine, new, old)]
    unnamed x1 -> x0, blocking collectives: 8.26 us -> none
  transfers between devices with their start and end apart: 7 -> 0, of which waited for: 3 -> 0; matrix products, arithmetic and copies ran while one was open for 36% -> 0% of each run, Pallas kernels for 0% -> 0%
where the time goes in v1:
time: 89.6 us; the launch traced here: 88.6 us
  Pallas kernels  81.9 us (91%)
  local copies, waits for them, and re-layouts  6.1 us (7%)
    pallas_call x1, Pallas kernels, body(): pl.pallas_call(functools.partial(step_kernel, ep, tp, stride, capacity),...  81.9 us
    unnamed x4, local copies, waits for them, and re-layouts  6.1 us

profile of v1, /device:TPU:1, one launch (start us, length us, event | category | flops | bytes accessed | tf_op | source)
XLA Modules:
  0.0 88.6 jit_solution(11128196091588521129)
XLA Ops:
  0.6 1.4 %copy.18.routes_ref = s32[64,2]{1,0:T(8,128)} copy(s32[64,2]{0,1:T(2,128)} %param.27) | data formatting | bytes 1024 | tf_op args[11]
  2.0 1.4 %copy.19.rw_ref = f32[64,2]{1,0:T(8,128)} copy(f32[64,2]{0,1:T(2,128)} %param.28) | data formatting | bytes 1024 | tf_op args[12]
  3.4 81.9 %shard_map.167 = (bf16[64,2048]{1,0:T(8,128)(2,1)}, bf16[64,2048]{1,0:T(8,128)(2,1)}) custom-call(bf16[256,256]{1,0:T(8,128)(2,1)} %q_ref.1, bf16[256,256]{1,0:T(8,128)(2,1)} %k_ref.1, bf16[256,512]{1,0:T(8,128)(2,1)} %v_ref.1, bf16[256,512]{1,0:T(8,128)(2,1)} %og_ref.1, f32[1,256]{1,0:T(1,128)} %ig_ref.1, f32[1,256]{1,0:T(1,128)} %fg_ref.1, ...), custom_call_target="tpu_custom_call" | custom-call | tf_op jit(solution)/shard_map/pallas_call | solution.py:418
  85.3 1.7 %copy.22 = bf16[64,2048]{1,0:T(8,128)(2,1)} copy(bf16[64,2048]{1,0:T(8,128)(2,1)} %get-tuple-element.4) | data formatting | bytes 524288
  87.0 1.7 %copy.23 = bf16[64,2048]{1,0:T(8,128)(2,1)} copy(bf16[64,2048]{1,0:T(8,128)(2,1)} %get-tuple-element.5) | data formatting | bytes 524288

commit v2 on v1

--- a/solution.py
+++ b/solution.py
@@ -104,11 +104,83 @@
     loads = [
         pltpu.make_async_copy(src, dst, w_sem.at[i])
         for i, (src, dst) in enumerate(
-            ((wo_hbm, wo), (wg_hbm.at[0], wg), (wu_hbm.at[0], wu), (wd_hbm.at[0], wd))
+            ((wg_hbm.at[0], wg), (wu_hbm.at[0], wu), (wd_hbm.at[0], wd), (wo_hbm, wo))
         )
     ]
     for load in loads:
         load.start()
+
+    x = tok_ref[...].astype(F32)
+    centre = jnp.mean(x, axis=1, keepdims=True)
+    spread = jnp.mean(jnp.square(x - centre), axis=1, keepdims=True)
+    normed = ((x - centre) * lax.rsqrt(spread + layer_eps) * egain_ref[...]).astype(BF16)
+    tok_r = lax.broadcasted_iota(jnp.int32, (tokens, tokens), 0)
+    tok_c = lax.broadcasted_iota(jnp.int32, (tokens, tokens), 1)
+
+    def column(row):
+        return jnp.sum(jnp.where(tok_r == tok_c, row, 0.0), axis=1, keepdims=True)
+
+    top = routes_ref.shape[0]
+    routes = [column(routes_ref[i : i + 1, :].astype(F32)).astype(jnp.int32) for i in range(top)]
+    lanes = max(128, -(-n // 128) * 128)
+    lane_e = lax.broadcasted_iota(jnp.int32, (tokens, lanes), 1)
+    hots = [(lane_e == routes[i]).astype(F32) for i in range(top)]
+    earlier = dot((tok_r > tok_c).astype(F32).astype(BF16), sum(hots).astype(BF16))
+    slot_i = lax.broadcasted_iota(jnp.int32, (tokens, n * stride), 1)
+    pick = jnp.zeros((tokens, n * stride), F32)
+    weigh = jnp.zeros((tokens, n * stride), F32)
+    for i in range(top):
+        place = jnp.sum(earlier * hots[i], axis=1, keepdims=True).astype(jnp.int32)
+        mine = (slot_i == routes[i] * stride + place).astype(F32)
+        pick = pick + mine
+        weigh = weigh + mine * column(rw_ref[i : i + 1, :])
+    comb[...] = weigh
+    pick = pick.astype(BF16)
+    out_rows[...] = dot(pick, normed, ((0,), (0,))).astype(BF16)
+
+    pl.semaphore_wait(barrier, n - 1)
+
+    def rows_of(ref, index):
+        return ref.at[pl.ds(pl.multiple_of(index * stride, row_tile), stride)]
+
+    def exchange(src, dst, send, recv, z2, t2, arriving):
+        p = z2 * tp + t2
+        return pltpu.make_async_remote_copy(
+            src_ref=rows_of(src, p),
+            dst_ref=rows_of(dst, p if arriving else me),
+            send_sem=send.at[p],
+            recv_sem=recv.at[p if arriving else me],
+            device_id=to(z2, t2),
+            device_id_type=pl.DeviceIdType.MESH,
+        )
+
+    def dispatch(z2, t2, arriving=False):
+        return exchange(out_rows, arrived, d_send, d_recv, z2, t2, arriving)
+
+    def give_back(z2, t2, arriving=False):
+        return exchange(results, returned, r_send, r_recv, z2, t2, arriving)
+
+    def each_peer(first, action, last=n):
+        def turn(i, c):
+            z2, t2 = peer(i // tp, lax.rem(i, tp))
+            action(z2, t2)
+            return c
+
+        lax.fori_loop(first, last, turn, 0)
+
+    own = pl.ds(pl.multiple_of(me * stride, row_tile), stride)
+
+    def chain(index, src, dst, z2):
+        return pltpu.make_async_remote_copy(
+            src_ref=src,
+            dst_ref=dst,
+            send_sem=c_send.at[index],
+            recv_sem=c_recv.at[index],
+            device_id=to(z2, t),
+            device_id_type=pl.DeviceIdType.MESH,
+        )
+
+    each_peer(1, lambda z2, t2: dispatch(z2, t2).start(), 2 * tp)
 
     rows_i = lax.broadcasted_iota(jnp.int32, (span, span), 0)
     cols_i = lax.broadcasted_iota(jnp.int32, (span, span), 1)
@@ -137,72 +209,6 @@
     fw_own[...] = dot((keys_f32 * jnp.exp(fw_w - fw_top)).astype(BF16), values, ((0,), (0,)))
     bw_own[...] = dot((keys_f32 * jnp.exp(bw_w - bw_top)).astype(BF16), values, ((0,), (0,)))
 
-    x = tok_ref[...].astype(F32)
-    centre = jnp.mean(x, axis=1, keepdims=True)
-    spread = jnp.mean(jnp.square(x - centre), axis=1, keepdims=True)
-    normed = ((x - centre) * lax.rsqrt(spread + layer_eps) * egain_ref[...]).astype(BF16)
-    routes = routes_ref[...]
-    lanes = max(128, -(-n // 128) * 128)
-    lane_e = lax.broadcasted_iota(jnp.int32, (tokens, lanes), 1)
-    top = routes.shape[1]
-    hots = [(lane_e == routes[:, i : i + 1]).astype(F32) for i in range(top)]
-    tok_r = lax.broadcasted_iota(jnp.int32, (tokens, tokens), 0)
-    tok_c = lax.broadcasted_iota(jnp.int32, (tokens, tokens), 1)
-    earlier = dot((tok_r > tok_c).astype(F32).astype(BF16), sum(hots).astype(BF16))
-    slot_i = lax.broadcasted_iota(jnp.int32, (tokens, n * stride), 1)
-    pick = jnp.zeros((tokens, n * stride), F32)
-    weigh = jnp.zeros((tokens, n * stride), F32)
-    for i in range(top):
-        place = jnp.sum(earlier * hots[i], axis=1, keepdims=True).astype(jnp.int32)
-        mine = (slot_i == routes[:, i : i + 1] * stride + place).astype(F32)
-        pick = pick + mine
-        weigh = weigh + mine * rw_ref[:, i : i + 1]
-    comb[...] = weigh
-    pick = pick.astype(BF16)
-    out_rows[...] = dot(pick, normed, ((0,), (0,))).astype(BF16)
-
-    pl.semaphore_wait(barrier, n - 1)
-
-    def rows_of(ref, index):
-        return ref.at[pl.ds(pl.multiple_of(index * stride, row_tile), stride)]
-
-    def exchange(src, dst, send, recv, z2, t2, arriving):
-        p = z2 * tp + t2
-        return pltpu.make_async_remote_copy(
-            src_ref=rows_of(src, p),
-            dst_ref=rows_of(dst, p if arriving else me),
-            send_sem=send.at[p],
-            recv_sem=recv.at[p if arriving else me],
-            device_id=to(z2, t2),
-            device_id_type=pl.DeviceIdType.MESH,
-        )
-
-    def dispatch(z2, t2, arriving=False):
-        return exchange(out_rows, arrived, d_send, d_recv, z2, t2, arriving)
-
-    def give_back(z2, t2, arriving=False):
-        return exchange(results, returned, r_send, r_recv, z2, t2, arriving)
-
-    def each_peer(first, action):
-        def turn(i, c):
-            z2, t2 = peer(i // tp, lax.rem(i, tp))
-            action(z2, t2)
-            return c
-
-        lax.fori_loop(first, n, turn, 0)
-
-    own = pl.ds(pl.multiple_of(me * stride, row_tile), stride)
-
-    def chain(index, src, dst, z2):
-        return pltpu.make_async_remote_copy(
-            src_ref=src,
-            dst_ref=dst,
-            send_sem=c_send.at[index],
-            recv_sem=c_recv.at[index],
-            device_id=to(z2, t),
-            device_id_type=pl.DeviceIdType.MESH,
-        )
-
     after = lax.rem(z + 1, ep)
     ahead = lax.rem(z + ep - 1, ep)
     fw_chain = (chain(0, fw_top_out, fw_top_in, after), chain(1, fw_out, fw_in, after))
@@ -247,22 +253,51 @@
                     copy.wait_recv()
 
             pass_on(bw_chain, bw_in, bw_top_in, bw_own, bw_top, bw_out, bw_top_out)
-
-        def plane(dt, c2):
-            z2, t2 = peer(s + 1, dt)
-            dispatch(z2, t2).start()
+        return c
+
+    lax.fori_loop(0, 1, stage, 0)
+    each_peer(2 * tp, lambda z2, t2: dispatch(z2, t2).start())
+    arrived[own] = out_rows[own]
+
+    fe = wg.shape[1]
+    cols = 256
+    plane_rows = tp * stride
+    for load in loads[:3]:
+        load.wait()
+
+    def expert_group(g):
+        first, last = max(1, 2 * g * tp), 2 * (g + 1) * tp
+        each_peer(first, lambda z2, t2: dispatch(z2, t2, True).wait_recv(), last)
+        near_at, far_at = [
+            pl.ds(pl.multiple_of(lax.rem(z + 2 * g + i, ep) * plane_rows, row_tile), plane_rows)
+            for i in range(2)
+        ]
+
+        def up(j, c2):
+            f = pl.ds(pl.multiple_of(j * cols, cols), cols)
+            rows = jnp.concatenate([arrived[near_at, :], arrived[far_at, :]], axis=0)
+            gate_part = dot(rows, wg[:, f])
+            up_part = dot(rows, wu[:, f])
+            hidden[:, f] = (gate_part * jax.nn.sigmoid(gate_part) * up_part).astype(BF16)
             return c2
 
-        return lax.fori_loop(0, tp, plane, c)
-
-    def near_plane(dt, c):
-        z2, t2 = peer(0, dt)
-        dispatch(z2, t2).start()
-        return c
-
-    lax.fori_loop(1, tp, near_plane, 0)
-    lax.fori_loop(0, ep - 1, stage, 0)
-    arrived[own] = out_rows[own]
+        lax.fori_loop(0, fe // cols, up, 0)
+
+        def down(j, c2):
+            f = pl.ds(pl.multiple_of(j * cols, cols), cols)
+            made = dot(hidden[...], wd[:, f]).astype(BF16)
+            results[near_at, f] = made[:plane_rows]
+            results[far_at, f] = made[plane_rows:]
+            return c2
+
+        lax.fori_loop(0, width // cols, down, 0)
+        each_peer(first, lambda z2, t2: give_back(z2, t2).start(), last)
+
+    groups = ep // 2
+    for g in range(groups):
+        lax.fori_loop(1 + g * (ep - 2) // groups, 1 + (g + 1) * (ep - 2) // groups, stage, 0)
+        expert_group(g)
+    returned[own] = results[own]
 
     from_row = through_col - through_row + in_row
     fw_log = jnp.where(lower, from_row, -jnp.inf)
@@ -296,8 +331,7 @@
     normed_rows = head_rows * lax.rsqrt(mean_square + norm_eps) * hgain_ref[...]
     gated[...] = (jax.nn.sigmoid(og_ref[...].astype(F32)) * normed_rows).astype(BF16)
 
-    loads[0].wait()
-    cols = 256
+    loads[3].wait()
 
     def project(i, c):
         at = pl.ds(pl.multiple_of(i * cols, cols), cols)
@@ -321,36 +355,6 @@
     for dt in range(1, tp):
         share(dt).start()
     parts_in[t] = parts_out[pl.ds(pl.multiple_of(t * sub, row_tile), sub), :]
-
-    for load in loads[1:]:
-        load.wait()
-    each_peer(1, lambda z2, t2: dispatch(z2, t2, True).wait_recv())
-    fe = wg.shape[1]
-    chunk = min(256, n * stride)
-
-    def expert_chunk(i, c):
-        at = pl.ds(pl.multiple_of(i * chunk, chunk), chunk)
-
-        def up(j, c2):
-            f = pl.ds(pl.multiple_of(j * cols, cols), cols)
-            rows = arrived[at, :]
-            gate_part = dot(rows, wg[:, f])
-            up_part = dot(rows, wu[:, f])
-            hidden[:, f] = (gate_part * jax.nn.sigmoid(gate_part) * up_part).astype(BF16)
-            return c2
-
-        lax.fori_loop(0, fe // cols, up, 0)
-
-        def down(j, c2):
-            f = pl.ds(pl.multiple_of(j * cols, cols), cols)
-            results[at, f] = dot(hidden[...], wd[:, f]).astype(BF16)
-            return c2
-
-        return lax.fori_loop(0, width // cols, down, c)
-
-    lax.fori_loop(0, n * stride // chunk, expert_chunk, 0)
-    each_peer(1, lambda z2, t2: give_back(z2, t2).start())
-    returned[own] = results[own]
 
     for dt in range(1, tp):
         share(dt, True).wait_recv()
@@ -446,7 +450,7 @@
             pltpu.VMEM((span, width), BF16),
             pltpu.VMEM((tp, span // tp, width), BF16),
             pltpu.VMEM((span, dv), BF16),
-            pltpu.VMEM((min(256, slots), fe), BF16),
+            pltpu.VMEM((2 * tp * stride, fe), BF16),
             dma((4,)),
             dma((n,)),
             dma((n,)),
@@ -472,8 +476,8 @@
         memory_output_matrix,
         expert_input_tokens,
         expert_norm_gain[None, :],
-        routes,
-        routed_expert_weight,
+        routes.T,
+        routed_expert_weight.T,
         expert_gate_matrix,
         expert_up_matrix,
         expert_down_matrix,

time: 89.6 us -> 76 us (0.85)
  Pallas kernels: 81.9 us -> 71.8 us
  local copies, waits for them, and re-layouts: 6.1 us -> 3.34 us
    pallas_call x1, Pallas kernels: 81.9 us -> 71.8 us  [body(): pl.pallas_call(functools.partial(step_kernel, ep, tp, stride, capacity),...]
    unnamed x4 -> x2, local copies, waits for them, and re-layouts: 6.1 us -> 3.34 us
where the time goes in v2:
time: 76 us; the launch traced here: 75.8 us
  Pallas kernels  71.8 us (94%)
  local copies, waits for them, and re-layouts  3.34 us (4%)
    pallas_call x1, Pallas kernels, body(): pl.pallas_call(functools.partial(step_kernel, ep, tp, stride, capacity),...  71.8 us
    unnamed x2, local copies, waits for them, and re-layouts  3.34 us

profile of v2, /device:TPU:1, one launch (start us, length us, event | category | flops | bytes accessed | tf_op | source)
XLA Modules:
  0.0 75.8 jit_solution(13103622063743186460)
XLA Ops:
  0.6 71.8 %shard_map.167 = (bf16[64,2048]{1,0:T(8,128)(2,1)}, bf16[64,2048]{1,0:T(8,128)(2,1)}) custom-call(bf16[256,256]{1,0:T(8,128)(2,1)} %q_ref.1, bf16[256,256]{1,0:T(8,128)(2,1)} %k_ref.1, bf16[256,512]{1,0:T(8,128)(2,1)} %v_ref.1, bf16[256,512]{1,0:T(8,128)(2,1)} %og_ref.1, f32[1,256]{1,0:T(1,128)} %ig_ref.1, f32[1,256]{1,0:T(1,128)} %fg_ref.1, ...), custom_call_target="tpu_custom_call" | custom-call | tf_op jit(solution)/shard_map/pallas_call | solution.py:422
  72.5 1.7 %copy.20 = bf16[64,2048]{1,0:T(8,128)(2,1)} copy(bf16[64,2048]{1,0:T(8,128)(2,1)} %get-tuple-element.4) | data formatting | bytes 524288
  74.1 1.7 %copy.21 = bf16[64,2048]{1,0:T(8,128)(2,1)} copy(bf16[64,2048]{1,0:T(8,128)(2,1)} %get-tuple-element.5) | data formatting | bytes 524288

commit v3 on v2

--- a/solution.py
+++ b/solution.py
@@ -41,8 +41,7 @@
     wg_hbm,
     wu_hbm,
     wd_hbm,
-    mix_ref,
-    exp_ref,
+    out_ref,
     wo,
     wg,
     wu,
@@ -260,7 +259,7 @@
     arrived[own] = out_rows[own]
 
     fe = wg.shape[1]
-    cols = 256
+    cols = 512
     plane_rows = tp * stride
     for load in loads[:3]:
         load.wait()
@@ -361,7 +360,7 @@
     mixed = parts_in[0].astype(F32)
     for i in range(1, tp):
         mixed = mixed + parts_in[i].astype(F32)
-    mix_ref[...] = mixed.astype(BF16)
+    out_ref[0:sub, :] = mixed.astype(BF16)
 
     weigh = comb[...]
     high = weigh.astype(BF16)
@@ -370,7 +369,7 @@
     for j in range(width // cols):
         f = slice(j * cols, (j + 1) * cols)
         rows = returned[:, f]
-        exp_ref[:, f] = (dot(high, rows) + dot(low, rows)).astype(BF16)
+        out_ref[sub : sub + tokens, f] = (dot(high, rows) + dot(low, rows)).astype(BF16)
 
     @pl.when(z < ep - 1)
     def _():
@@ -419,14 +418,11 @@
     vmem = pl.BlockSpec(memory_space=pltpu.VMEM)
     hbm = pl.BlockSpec(memory_space=pl.ANY)
     dma = pltpu.SemaphoreType.DMA
-    return pl.pallas_call(
+    both = pl.pallas_call(
         functools.partial(step_kernel, ep, tp, stride, capacity),
-        out_shape=(
-            jax.ShapeDtypeStruct((span // tp, width), BF16),
-            jax.ShapeDtypeStruct((tokens, width), BF16),
-        ),
+        out_shape=jax.ShapeDtypeStruct((span // tp + tokens, width), BF16),
         in_specs=[vmem] * 8 + [hbm] + [vmem] * 4 + [hbm] * 3,
-        out_specs=(vmem, vmem),
+        out_specs=vmem,
         scratch_shapes=[
             pltpu.VMEM((dv, width), BF16),
             pltpu.VMEM((width, fe), BF16),
@@ -482,6 +478,7 @@
         expert_up_matrix,
         expert_down_matrix,
     )
+    return both[: span // tp], both[span // tp :]
 
 
 def solution(mesh):

time: 76 us -> 73.6 us (0.968)
  local copies, waits for them, and re-layouts: 3.34 us -> 1.87 us
  Pallas kernels: 71.8 us -> 71 us
    unnamed x2 -> x0, local copies, waits for them, and re-layouts: 3.34 us -> none
    slice x0 -> x1, local copies, waits for them, and re-layouts: none -> 1.87 us  [body(): return (both[:span // tp], both[span // tp:])]
    pallas_call x1, Pallas kernels: 71.8 us -> 71 us  [body(): pl.pallas_call(functools.partial(step_kernel, ep, tp, stride, capacity),...]
where the time goes in v3:
time: 73.6 us; the launch traced here: 73.5 us
  Pallas kernels  71 us (96%)
  local copies, waits for them, and re-layouts  1.87 us (3%)
    pallas_call x1, Pallas kernels, body(): pl.pallas_call(functools.partial(step_kernel, ep, tp, stride, capacity),...  71 us
    slice x1, local copies, waits for them, and re-layouts, body(): return (both[:span // tp], both[span // tp:])  1.87 us

profile of v3, /device:TPU:1, one launch (start us, length us, event | category | flops | bytes accessed | tf_op | source)
XLA Modules:
  0.0 73.5 jit_solution(6057638898464619458)
XLA Ops:
  0.6 71.0 %shard_map.167 = bf16[128,2048]{1,0:T(8,128)(2,1)} custom-call(bf16[256,256]{1,0:T(8,128)(2,1)} %q_ref.1, bf16[256,256]{1,0:T(8,128)(2,1)} %k_ref.1, bf16[256,512]{1,0:T(8,128)(2,1)} %v_ref.1, bf16[256,512]{1,0:T(8,128)(2,1)} %og_ref.1, f32[1,256]{1,0:T(1,128)} %ig_ref.1, f32[1,256]{1,0:T(1,128)} %fg_ref.1, f32[1,256]{1,0:T(1,128)} %xf_ref.1, ...), custom_call_target="tpu_custom_call" | custom-call | tf_op jit(solution)/shard_map/pallas_call | solution.py:421
  71.6 1.9 %fusion = (bf16[64,2048]{1,0:T(8,128)(2,1)}, bf16[64,2048]{1,0:T(8,128)(2,1)}) fusion(bf16[128,2048]{1,0:T(8,128)(2,1)} %shard_map.167), kind=kLoop, calls=%fused_computation | loop fusion | bytes 1048576 | tf_op jit(solution)/shard_map/slice | solution.py:481
